TPU v7x, 32 devices: a whole 2x2x4 slice. The times are simulated.
32 devices in a mesh: ep: 8 (over z, x), tp: 4 (over y, core).
Axes of the slice: x: 2, y: 2, z: 4, core: 2. Of those that a mesh axis runs over, the one named last changes fastest.
Arguments:
- tokens: bfloat16 [192, 4096], P('ep'), may hold values from -6 to 6
- delta_state: float32 [192, 16, 128, 128], P('ep', 'tp'), may hold values from -0.625 to 0.625
- attn_gain: float32 [4096], replicated, may hold values from 0.1 to 1.9
- query_weight: bfloat16 [4096, 2048], P('ep', 'tp'), may hold values from -0.09375 to 0.09375
- key_weight: bfloat16 [4096, 2048], P('ep', 'tp'), may hold values from -0.09375 to 0.09375
- value_weight: bfloat16 [4096, 2048], P('ep', 'tp'), may hold values from -0.09375 to 0.09375
- decay_weight: bfloat16 [4096, 16], replicated, may hold values from -0.09375 to 0.09375
- beta_weight: bfloat16 [4096, 16], replicated, may hold values from -0.09375 to 0.09375
- decay_rate: float32 [16], P('tp'), may hold values from 0.05 to 3
- head_gain: float32 [128], replicated, may hold values from 0.1 to 1.9
- output_weight: bfloat16 [2048, 4096], P('tp'), may hold values from -0.125 to 0.125
- ffn_gain: float32 [4096], replicated, may hold values from 0.1 to 1.9
- expert_ids: int32 [192, 2], P('ep'), may hold values from 0 to 7, all different within a row; in each aligned block of 24 rows (0 to 23, 24 to 47, ...) at most 12 rows name the same one
- group_prob: float32 [192], P('ep'), may hold values from 0.3 to 1
- expert_logit: float32 [192, 2], P('ep'), may hold values from -8 to 8
- expert_gate: bfloat16 [8, 4096, 1024], P('ep', None, 'tp'), may hold values from -0.09375 to 0.09375
- expert_up: bfloat16 [8, 4096, 1024], P('ep', None, 'tp'), may hold values from -0.09375 to 0.09375
- expert_down: bfloat16 [8, 1024, 4096], P('ep', 'tp'), may hold values from -0.1875 to 0.1875
- dense_gate: bfloat16 [4096, 4096], P('tp', 'ep'), may hold values from -0.09375 to 0.09375
- dense_up: bfloat16 [4096, 4096], P('tp', 'ep'), may hold values from -0.09375 to 0.09375
- dense_down: bfloat16 [4096, 4096], P('ep', 'tp'), may hold values from -0.09375 to 0.09375
- dense_mix: float32 [4096], P('tp'), may hold values from -3 to 3
Outputs:
- mixed_out: bfloat16 [192, 4096], P('ep', 'tp')
- new_state: float32 [192, 16, 128, 128], P('ep', 'tp')
Inputs may be any that keep to these rules, and one draw needn't show every extreme that they name: `expert_ids`: each row names 2 different experts. Among the rows of one device (aligned blocks of 24 rows) no expert is named by more than 12 rows, and in every draw some expert reaches 12 in some block.
All inputs are finite; a program needn't handle non-finite values.
Results may differ from a plain program's by a relative error of at most 0.02.
Values may be sent and summed in bfloat16 or wider, within the bound.
A program may use at most 64 MiB of HBM per device.

v0:
```python
import jax
import jax.numpy as jnp
from jax import lax
from jax.sharding import PartitionSpec as P

EPS = 1e-06


def rms_scale(values, gain):
    mean_sq = jnp.mean(values * values, axis=-1, keepdims=True)
    return values * lax.rsqrt(mean_sq + EPS) * gain


def unit_rows(values):
    return values * lax.rsqrt(jnp.sum(values * values, axis=-1, keepdims=True) + EPS)


def per_device(
    tokens,
    delta_state,
    attn_gain,
    query_weight,
    key_weight,
    value_weight,
    decay_weight,
    beta_weight,
    decay_rate,
    head_gain,
    output_weight,
    ffn_gain,
    expert_ids,
    group_prob,
    expert_logit,
    expert_gate,
    expert_up,
    expert_down,
    dense_gate,
    dense_up,
    dense_down,
    dense_mix,
):
    seq_rows = tokens.shape[0]
    head_count = delta_state.shape[1]
    head_size = delta_state.shape[2]
    width_local = head_count * head_size
    tp_index = lax.axis_index("tp")
    residual = tokens.astype(jnp.float32)
    normed = rms_scale(residual, attn_gain).astype(jnp.bfloat16)
    spread = lax.all_to_all(normed, "ep", split_axis=1, concat_axis=0, tiled=True)
    joined = jnp.concatenate((query_weight, key_weight, value_weight), axis=1)
    summed = lax.psum_scatter(
        jnp.dot(spread, joined, preferred_element_type=jnp.float32).astype(jnp.bfloat16),
        "ep",
        scatter_dimension=0,
        tiled=True,
    ).astype(jnp.float32)
    query_sum = summed[:, :width_local]
    key_sum = summed[:, width_local : 2 * width_local]
    value_sum = summed[:, 2 * width_local :]

    def heads_of(values):
        rounded = lax.optimization_barrier(values.astype(jnp.bfloat16))
        return rounded.astype(jnp.float32).reshape(seq_rows, head_count, head_size)

    query_unit = unit_rows(heads_of(query_sum)) * head_size ** (-0.5)
    key_unit = unit_rows(heads_of(key_sum))
    value_heads = heads_of(value_sum)
    decay_cols = lax.dynamic_slice_in_dim(decay_weight, tp_index * head_count, head_count, 1)
    beta_cols = lax.dynamic_slice_in_dim(beta_weight, tp_index * head_count, head_count, 1)
    decay_pre = jnp.dot(normed, decay_cols, preferred_element_type=jnp.float32)
    decay = jnp.exp(-decay_rate * jax.nn.softplus(decay_pre))
    beta_gate = jax.nn.sigmoid(jnp.dot(normed, beta_cols, preferred_element_type=jnp.float32))
    recalled = jnp.einsum("bhk,bhkv->bhv", key_unit, delta_state, precision=lax.Precision.HIGHEST)
    correction = beta_gate[..., None] * (value_heads - decay[..., None] * recalled)
    new_state = (
        decay[..., None, None] * delta_state + key_unit[..., :, None] * correction[..., None, :]
    )
    read_out = jnp.einsum("bhk,bhkv->bhv", query_unit, new_state, precision=lax.Precision.HIGHEST)
    head_out = rms_scale(read_out, head_gain).astype(jnp.bfloat16).reshape(seq_rows, width_local)
    attn_part = jnp.dot(head_out, output_weight, preferred_element_type=jnp.float32)
    attn_sum = lax.psum(attn_part.astype(jnp.bfloat16), "tp").astype(jnp.float32)
    middle = residual + attn_sum
    ffn_in = rms_scale(middle, ffn_gain).astype(jnp.bfloat16)
    slice_width = dense_gate.shape[0]
    hidden_width = dense_gate.shape[1]
    own_columns = lax.dynamic_slice_in_dim(ffn_in, tp_index * slice_width, slice_width, 1)
    gate_up = jnp.concatenate((dense_gate, dense_up), axis=1)
    dense_part = jnp.dot(
        lax.all_gather(own_columns, "ep", axis=0, tiled=True),
        gate_up,
        preferred_element_type=jnp.float32,
    )
    dense_sum = lax.psum(dense_part.astype(jnp.bfloat16), "tp").astype(jnp.float32)
    dense_hidden = (jax.nn.silu(dense_sum[:, :hidden_width]) * dense_sum[:, hidden_width:]).astype(
        jnp.bfloat16
    )
    dense_out = lax.psum_scatter(
        jnp.dot(dense_hidden, dense_down, preferred_element_type=jnp.float32).astype(jnp.bfloat16),
        "ep",
        scatter_dimension=0,
        tiled=True,
    ).astype(jnp.float32)
    expert_count = lax.axis_size("ep")
    top_count = expert_ids.shape[1]
    capacity = max(2, 2 * seq_rows * top_count // expert_count)
    pair_ids = expert_ids.reshape(-1)
    onehot = (pair_ids[:, None] == jnp.arange(expert_count, dtype=jnp.int32)[None, :]).astype(
        jnp.int32
    )
    ranks = jnp.sum(onehot * (jnp.cumsum(onehot, axis=0) - 1), axis=1)
    places = pair_ids * capacity + ranks
    dispatch = (
        jnp.arange(expert_count * capacity, dtype=jnp.int32)[:, None] == places[None, :]
    ).astype(jnp.bfloat16)
    repeated = jnp.repeat(ffn_in, top_count, axis=0)
    outgoing = jnp.dot(dispatch, repeated, preferred_element_type=jnp.float32).astype(jnp.bfloat16)
    outgoing = outgoing.reshape(expert_count, capacity, ffn_in.shape[1])
    arrived = lax.all_to_all(outgoing, "ep", split_axis=0, concat_axis=0, tiled=True)
    gate_vals = jnp.einsum(
        "snd,df->snf", arrived, expert_gate[0], preferred_element_type=jnp.float32
    )
    up_vals = jnp.einsum("snd,df->snf", arrived, expert_up[0], preferred_element_type=jnp.float32)
    expert_hidden = (jax.nn.silu(gate_vals) * up_vals).astype(jnp.bfloat16)
    partial_value = jnp.einsum(
        "snf,fd->snd", expert_hidden, expert_down[0], preferred_element_type=jnp.float32
    )
    summed_cols = lax.psum_scatter(
        partial_value.astype(jnp.bfloat16), "tp", scatter_dimension=2, tiled=True
    )
    returned = lax.all_to_all(summed_cols, "ep", split_axis=0, concat_axis=0, tiled=True)
    flat_back = returned.reshape(expert_count * capacity, slice_width)
    picked = (
        jnp.take(flat_back, places, axis=0)
        .astype(jnp.float32)
        .reshape(seq_rows, top_count, slice_width)
    )
    logit_exp = jnp.exp(expert_logit)
    route_weight = group_prob[:, None] * logit_exp / jnp.sum(logit_exp, axis=1, keepdims=True)
    expert_mix = jnp.sum(route_weight[..., None] * picked, axis=1)
    own_middle = lax.dynamic_slice_in_dim(middle, tp_index * slice_width, slice_width, 1)
    mixed_out = (own_middle + jax.nn.sigmoid(dense_mix) * dense_out + expert_mix).astype(
        jnp.bfloat16
    )
    return (mixed_out, new_state)


def solution(mesh):
    return jax.shard_map(
        per_device,
        mesh=mesh,
        in_specs=(
            P("ep", None),
            P("ep", "tp", None, None),
            P(),
            P("ep", "tp"),
            P("ep", "tp"),
            P("ep", "tp"),
            P(),
            P(),
            P("tp"),
            P(),
            P("tp", None),
            P(),
            P("ep", None),
            P("ep"),
            P("ep", None),
            P("ep", None, "tp"),
            P("ep", None, "tp"),
            P("ep", "tp", None),
            P("tp", "ep"),
            P("tp", "ep"),
            P("ep", "tp"),
            P("tp"),
        ),
        out_specs=(P("ep", "tp"), P("ep", "tp", None, None)),
        check_vma=False,
    )
```

profile of v0, /device:TPU:0, one launch (start us, length us, event | category | flops | bytes accessed | tf_op | source)
XLA Modules:
  0.0 333.8 jit_solution(11705922929324244987)
XLA Ops:
  7.2 1.2 fusion.28
  8.4 1.1 fusion.30
  9.6 15.0 %all_to_all.29 = bf16[24,8,512]{2,0,1:T(8,128)(2,1)S(1)} all-to-all(bf16[24,8,512]{2,0,1:T(8,128)(2,1)S(1)} %bitcast.59), channel_id=1, replica_groups=mesh['ep'=8,'tp'=4] {'ep'}, dimensions={1} | all-to-all | bytes 393216 | tf_op jit(solution)/shard_map/all_to_all | solution.py:49
  24.6 2.7 convolution_convert_fusion.3
  27.4 1.0 fusion.48
  28.4 0.1 copy.67
  28.5 1.0 fusion.27
  29.5 0.1 copy.68
  29.6 0.1 copy.73
  29.7 0.1 reshape.151
  30.0 0.2 select_reduce_fusion
  30.1 58.6 %reduce-scatter.4.cloned.1.call-done = bf16[24,1536]{1,0:T(8,128)(2,1)} async-done(((bf16[192,1536]{1,0:T(8,128)(2,1)}), bf16[24,1536]{1,0:T(8,128)(2,1)}) %reduce-scatter.4.cloned.1.call-update) | async-done | bytes 73744 | tf_op jit(solution)/shard_map/reduce_scatter | solution.py:51
  88.8 0.8 fusion.58
  89.6 0.1 multiply_reduce_fusion.3
  89.7 0.1 broadcast_multiply_fusion
  89.8 8.1 %fusion.59 = f32[24,4,1,128]{3,2,1,0:T(1,128)S(1)} fusion(f32[24,4,128,1]{2,3,1,0:T(1,128)S(1)} %bitcast.60, f32[24,4,128,128]{3,2,1,0:T(8,128)} %param.23), kind=kOutput, calls=%fused_computation.93 | convolution fusion | flops 18874368 | bytes 6389760 | tf_op jit(solution)/shard_map/bhk,bhkv->bhv/dot_general | solution.py:73
  97.9 0.1 subtract_multiply_fusion
  98.1 3.9 %multiply_add_fusion = f32[24,4,128,128]{3,2,1,0:T(8,128)} fusion(f32[24,4,128,128]{3,2,1,0:T(8,128)S(1)} %copy-done.1, f32[24,4,128]{2,1,0:T(4,128)S(1)} %subtract_multiply_fusion, f32[24,4,128]{2,1,0:T(4,128)S(1)} %broadcast_multiply_fusion, f32[24,4]{1,0:T(8,128)S(1)} %copy.67), kind=kLoop, calls=%fused_computation.1 | loop fusion | flops 4718592 | bytes 12681600 | tf_op jit(solution)/shard_map/add | solution.py:76
  101.9 0.1 multiply_reduce_fusion.4
  102.1 0.1 multiply_multiply_fusion
  102.2 7.5 %fusion.60 = f32[24,4,1,128]{3,2,1,0:T(1,128)S(1)} fusion(f32[24,4,128,1]{2,3,1,0:T(1,128)S(1)} %bitcast.63, f32[24,4,128,128]{3,2,1,0:T(8,128)} %multiply_add_fusion), kind=kOutput, calls=%fused_computation.94 | convolution fusion | flops 18874368 | bytes 6389760 | tf_op jit(solution)/shard_map/bhk,bhkv->bhv/dot_general | solution.py:78
  109.7 0.1 multiply_reduce_fusion.2
  109.8 0.1 multiply_convert_fusion.1
  109.9 1.4 convolution_convert_fusion.2
  111.3 31.2 %all-reduce.3.cloned.1.call-done = bf16[24,4096]{1,0:T(8,128)(2,1)} async-done(((bf16[24,4096]{1,0:T(8,128)(2,1)}), bf16[24,4096]{1,0:T(8,128)(2,1)}) %all-reduce.3.cloned.1.call-update) | async-done | bytes 196624 | tf_op jit(solution)/shard_map/psum | solution.py:81
  142.5 1.8 convert_add_fusion
  144.3 1.0 multiply_convert_fusion
  145.4 0.3 broadcast_in_dim.10
  145.7 0.2 reshape.152
  145.9 0.3 convolution_convert_fusion.1
  146.2 1.2 reshape.153
  147.4 5.5 %all-to-all-start.1 = ((bf16[8,12,4096]{2,1,0:T(8,128)(2,1)}), bf16[8,12,4096]{2,1,0:T(8,128)(2,1)S(1)}, u32[]{:S(2)}, u32[]{:S(2)}) async-start(bf16[8,12,4096]{2,1,0:T(8,128)(2,1)} %reshape.153), calls=%async_computation.3 | async-start | bytes 2097152 | tf_op jit(solution)/shard_map/all_to_all | solution.py:118
  153.0 45.7 %all_gather.3 = bf16[192,1024]{1,0:T(8,128)(2,1)S(1)} all-gather(bf16[24,1024]{1,0:T(8,128)(2,1)S(1)} %constant_dynamic-slice_fusion), channel_id=1, replica_groups=mesh['ep'=8,'tp'=4] {'ep'}, dimensions={0}, use_global_device_ids=true | all-gather | bytes 442368 | tf_op jit(solution)/shard_map/all_gather | solution.py:89
  198.6 2.9 fusion.14
  201.6 2.0 fusion.7
  203.7 3.9 %convolution_convert_fusion = bf16[8,12,4096]{2,1,0:T(8,128)(2,1)} fusion(bf16[1,256,4096]{2,1,0:T(8,128)(2,1)S(1)} %copy-done, bf16[8,12,4096]{2,1,0:T(8,128)(2,1)S(1)} %all-to-all-done.1, bf16[1,4096,256]{2,1,0:T(8,128)(2,1)} %param.38, f32[8,12,256]{2,1,0:T(8,128)S(1)} %fusion.7), kind=kOutput, calls=%fused_computation.2 | convolution fusion | flops 403193856 | bytes 5865472 | tf_op jit(solution)/shard_map/snf,fd->snd/dot_general | solution.py:124
  207.9 25.3 %all-reduce.5.cloned.1.call-done = bf16[192,1024]{1,0:T(8,128)(2,1)} async-done(((bf16[192,1024]{1,0:T(8,128)(2,1)}), bf16[192,1024]{1,0:T(8,128)(2,1)}) %all-reduce.5.cloned.1.call-update) | async-done | bytes 393232 | tf_op jit(solution)/shard_map/psum | solution.py:93
  233.2 1.1 convert_element_type.71
  234.3 2.4 convolution_convert_fusion.4
  236.8 0.1 mul.260
  236.9 23.5 %reduce-scatter.8.cloned.1.call-done = bf16[8,12,1024]{2,1,0:T(8,128)(2,1)} async-done(((bf16[8,12,4096]{2,1,0:T(8,128)(2,1)}), bf16[8,12,1024]{2,1,0:T(8,128)(2,1)}) %reduce-scatter.8.cloned.1.call-update) | async-done | bytes 196624 | tf_op jit(solution)/shard_map/reduce_scatter | solution.py:127
  260.4 5.5 %all-to-all-start.2 = ((bf16[8,12,1024]{2,1,0:T(8,128)(2,1)}), bf16[8,12,1024]{2,1,0:T(8,128)(2,1)S(1)}, u32[]{:S(2)}, u32[]{:S(2)}) async-start(bf16[8,12,1024]{2,1,0:T(8,128)(2,1)} %reduce-scatter.8.cloned.1.call-done), calls=%async_computation.5 | async-start | bytes 524288 | tf_op jit(solution)/shard_map/all_to_all | solution.py:130
  265.9 0.1 copy.75
  266.1 9.1 %all-to-all-done.2 = bf16[8,12,1024]{2,1,0:T(8,128)(2,1)S(1)} async-done(((bf16[8,12,1024]{2,1,0:T(8,128)(2,1)}), bf16[8,12,1024]{2,1,0:T(8,128)(2,1)S(1)}, u32[]{:S(2)}, u32[]{:S(2)}) %all-to-all-start.2) | async-done | bytes 196640 | tf_op jit(solution)/shard_map/all_to_all | solution.py:130
  275.2 0.7 gather_fusion
  276.0 0.4 multiply_reduce_fusion.1
  276.4 49.3 %reduce-scatter.6.cloned.1.call-done = bf16[24,1024]{1,0:T(8,128)(2,1)} async-done(((bf16[192,1024]{1,0:T(8,128)(2,1)}), bf16[24,1024]{1,0:T(8,128)(2,1)}) %reduce-scatter.6.cloned.1.call-update) | async-done | bytes 49168 | tf_op jit(solution)/shard_map/reduce_scatter | solution.py:97
  325.7 1.6 add_convert_fusion
  (60 shorter events, 1.1 us)
Async XLA Ops:
  7.2 196.5 %copy-start = (bf16[1,256,4096]{2,1,0:T(8,128)(2,1)S(1)}, bf16[1,256,4096]{2,1,0:T(8,128)(2,1)}, u32[]{:S(2)}) copy-start(bf16[1,256,4096]{2,1,0:T(8,128)(2,1)} %param.39) | copy-start | bytes 6291460
  7.2 81.6 %reduce-scatter.4.cloned.1.call-start = ((), (), s32[]{:S(2)}) async-start(), calls=%async_computation.6 | async-start | bytes 663552 | tf_op jit(solution)/shard_map/reduce_scatter | solution.py:51
  9.5 17.8 %copy-start.10 = (f32[4]{0:T(128)S(1)}, f32[4]{0:T(128)}, u32[]{:S(2)}) copy-start(f32[4]{0:T(128)} %param.30) | copy-start | bytes 52
  9.5 20.1 %copy-start.5 = (s32[24,2]{0,1:T(2,128)S(1)}, s32[24,2]{0,1:T(2,128)}, u32[]{:S(2)}) copy-start(s32[24,2]{0,1:T(2,128)} %param.34) | copy-start | bytes 580
  27.3 115.2 %all-reduce.3.cloned.1.call-start = ((), (), s32[]{:S(2)}) async-start(), calls=%async_computation.7 | async-start | bytes 393216 | tf_op jit(solution)/shard_map/psum | solution.py:81
  89.8 8.2 %copy-start.1 = (f32[24,4,128,128]{3,2,1,0:T(8,128)S(1)}, f32[24,4,128,128]{3,2,1,0:T(8,128)}, u32[]{:S(2)}) copy-start(f32[24,4,128,128]{3,2,1,0:T(8,128)} %param.23) | copy-start | bytes 18874372
  102.2 7.6 %copy-start.8 = (f32[128]{0:T(128)S(1)}, f32[128]{0:T(128)}, u32[]{:S(2)}) copy-start(f32[128]{0:T(128)} %param.31) | copy-start | bytes 1540
  102.2 7.7 %copy-start.2 = (bf16[512,4096]{1,0:T(8,128)(2,1)S(1)}, bf16[512,4096]{1,0:T(8,128)(2,1)}, u32[]{:S(2)}) copy-start(bf16[512,4096]{1,0:T(8,128)(2,1)} %param.32) | copy-start | bytes 12582916
  109.7 32.8 %copy-start.3 = (bf16[24,4096]{1,0:T(8,128)(2,1)S(1)}, bf16[24,4096]{1,0:T(8,128)(2,1)}, u32[]{:S(2)}) copy-start(bf16[24,4096]{1,0:T(8,128)(2,1)} %param.22) | copy-start | bytes 589828
  109.7 34.7 %copy-start.4 = (f32[4096]{0:T(1024)S(1)}, f32[4096]{0:T(1024)}, u32[]{:S(2)}) copy-start(f32[4096]{0:T(1024)} %param.33) | copy-start | bytes 49156
  147.4 54.2 %all-to-all-start.1 = ((bf16[8,12,4096]{2,1,0:T(8,128)(2,1)}), bf16[8,12,4096]{2,1,0:T(8,128)(2,1)S(1)}, u32[]{:S(2)}, u32[]{:S(2)}) async-start(bf16[8,12,4096]{2,1,0:T(8,128)(2,1)} %reshape.153), calls=%async_computation.3 | async-start | bytes 2097152 | tf_op jit(solution)/shard_map/all_to_all | solution.py:118
  152.9 80.3 %all-reduce.5.cloned.1.call-start = ((), (), s32[]{:S(2)}) async-start(), calls=%async_computation.8 | async-start | bytes 786432 | tf_op jit(solution)/shard_map/psum | solution.py:93
  201.5 58.9 %reduce-scatter.8.cloned.1.call-start = ((), (), s32[]{:S(2)}) async-start(), calls=%async_computation.10 | async-start | bytes 1310720 | tf_op jit(solution)/shard_map/reduce_scatter | solution.py:127
  203.7 4.2 %copy-start.7 = (f32[24,2]{0,1:T(2,128)S(1)}, f32[24,2]{0,1:T(2,128)}, u32[]{:S(2)}) copy-start(f32[24,2]{0,1:T(2,128)} %param.36) | copy-start | bytes 580
  203.7 4.2 %copy-start.9 = (f32[24]{0:T(128)S(1)}, f32[24]{0:T(128)}, u32[]{:S(2)}) copy-start(f32[24]{0:T(128)} %param.35) | copy-start | bytes 292
  207.6 58.5 %copy-start.6 = (f32[1024]{0:T(1024)S(1)}, f32[1024]{0:T(1024)}, u32[]{:S(2)}) copy-start(f32[1024]{0:T(1024)} %param.43) | copy-start | bytes 12292
  207.6 118.1 %reduce-scatter.6.cloned.1.call-start = ((), (), s32[]{:S(2)}) async-start(), calls=%async_computation.9 | async-start | bytes 442368 | tf_op jit(solution)/shard_map/reduce_scatter | solution.py:97
  260.4 14.8 %all-to-all-start.2 = ((bf16[8,12,1024]{2,1,0:T(8,128)(2,1)}), bf16[8,12,1024]{2,1,0:T(8,128)(2,1)S(1)}, u32[]{:S(2)}, u32[]{:S(2)}) async-start(bf16[8,12,1024]{2,1,0:T(8,128)(2,1)} %reduce-scatter.8.cloned.1.call-done), calls=%async_computation.5 | async-start | bytes 524288 | tf_op jit(solution)/shard_map/all_to_all | solution.py:130
Sparse Core Ops, SparseCore 0:
  27.4 61.3 reduce-scatter.3
  111.4 31.0 all-reduce.2
  201.7 31.4 all-reduce.4
  235.6 24.7 reduce-scatter.7
  263.5 62.1 reduce-scatter.5
where the time goes:
time: 335 us; the launch traced here: 334 us
  waiting for transfers between devices  197 us (59%)
  blocking collectives  60.7 us (18%)
  matrix products  33.2 us (10%)
  between operations  14.1 us (4%)
  other arithmetic  13.2 us (4%)
  starting transfers between devices  11.2 us (3%)
  local copies, waits for them, and re-layouts  4.25 us (1%)
    reduce_scatter x1, waiting for transfers between devices, per_device(): lax.psum_scatter(jnp.dot(spread, joined, preferred_element_type=jnp.float...  58.6 us
    reduce_scatter x1, waiting for transfers between devices, per_device(): lax.psum_scatter(jnp.dot(dense_hidden, dense_down, preferred_element_type...  49.3 us
    all_gather x1, blocking collectives, per_device(): lax.all_gather(own_columns, 'ep', axis=0, tiled=True)  45.7 us
    psum x1, waiting for transfers between devices, per_device(): lax.psum(attn_part.astype(jnp.bfloat16), 'tp').astype(jnp.float32)  31.2 us
    psum x1, waiting for transfers between devices, per_device(): lax.psum(dense_part.astype(jnp.bfloat16), 'tp').astype(jnp.float32)  25.3 us
    reduce_scatter x1, waiting for transfers between devices, per_device(): lax.psum_scatter(partial_value.astype(jnp.bfloat16), 'tp', scatter_dimens...  23.5 us
    all_to_all x1, blocking collectives, per_device(): lax.all_to_all(normed, 'ep', split_axis=1, concat_axis=0, tiled=True)  15 us
    all_to_all x1, waiting for transfers between devices, per_device(): lax.all_to_all(summed_cols, 'ep', split_axis=0, concat_axis=0, tiled=True)  9.06 us
  transfers between devices with their start and end apart: 7, of which 6 were waited for; matrix products, arithmetic and copies ran while one was open for 5% of the time, Pallas kernels for 0%

commit v1 on v0

--- a/solution.py
+++ b/solution.py
@@ -78,7 +78,9 @@
     read_out = jnp.einsum("bhk,bhkv->bhv", query_unit, new_state, precision=lax.Precision.HIGHEST)
     head_out = rms_scale(read_out, head_gain).astype(jnp.bfloat16).reshape(seq_rows, width_local)
     attn_part = jnp.dot(head_out, output_weight, preferred_element_type=jnp.float32)
-    attn_sum = lax.psum(attn_part.astype(jnp.bfloat16), "tp").astype(jnp.float32)
+    attn_sum = jnp.sum(lax.all_gather(attn_part.astype(jnp.bfloat16), "tp"), axis=0).astype(
+        jnp.float32
+    )
     middle = residual + attn_sum
     ffn_in = rms_scale(middle, ffn_gain).astype(jnp.bfloat16)
     slice_width = dense_gate.shape[0]

time: 335 us -> 309 us (0.922)
  waiting for transfers between devices: 197 us -> 166 us
  blocking collectives: 60.7 us -> 70.9 us
    psum x1 -> x0, waiting for transfers between devices: 31.2 us -> none  [per_device(): lax.psum(attn_part.astype(jnp.bfloat16), 'tp').astype(jnp.float32)]
    all_gather x0 -> x1, blocking collectives: none -> 8.59 us  [per_device(): lax.all_gather(attn_part.astype(jnp.bfloat16), 'tp')]
  transfers between devices with their start and end apart: 7 -> 6, of which waited for: 6 -> 5; matrix products, arithmetic and copies ran while one was open for 5% -> 5% of each run, Pallas kernels for 0% -> 0%
where the time goes in v1:
time: 309 us; the launch traced here: 308 us
  waiting for transfers between devices  166 us (54%)
  blocking collectives  70.9 us (23%)
  matrix products  32.5 us (11%)
  between operations  14.2 us (5%)
  other arithmetic  11.5 us (4%)
  starting transfers between devices  9.31 us (3%)
  local copies, waits for them, and re-layouts  4.26 us (1%)
    reduce_scatter x1, waiting for transfers between devices, per_device(): lax.psum_scatter(jnp.dot(spread, joined, preferred_element_type=jnp.float...  58.6 us
    reduce_scatter x1, waiting for transfers between devices, per_device(): lax.psum_scatter(jnp.dot(dense_hidden, dense_down, preferred_element_type...  49.3 us
    all_gather x1, blocking collectives, per_device(): lax.all_gather(own_columns, 'ep', axis=0, tiled=True)  47.3 us
    psum x1, waiting for transfers between devices, per_device(): lax.psum(dense_part.astype(jnp.bfloat16), 'tp').astype(jnp.float32)  24.8 us
    reduce_scatter x1, waiting for transfers between devices, per_device(): lax.psum_scatter(partial_value.astype(jnp.bfloat16), 'tp', scatter_dimens...  23.7 us
    all_to_all x1, blocking collectives, per_device(): lax.all_to_all(normed, 'ep', split_axis=1, concat_axis=0, tiled=True)  15 us
    all_to_all x1, waiting for transfers between devices, per_device(): lax.all_to_all(summed_cols, 'ep', split_axis=0, concat_axis=0, tiled=True)  9.06 us
    all_gather x1, blocking collectives, per_device(): lax.all_gather(attn_part.astype(jnp.bfloat16), 'tp')  8.59 us
  transfers between devices with their start and end apart: 6, of which 5 were waited for; matrix products, arithmetic and copies ran while one was open for 5% of the time, Pallas kernels for 0%

profile of v1, /device:TPU:0, one launch (start us, length us, event | category | flops | bytes accessed | tf_op | source)
XLA Modules:
  0.0 308.2 jit_solution(13727031036999905464)
XLA Ops:
  7.2 1.2 fusion.28
  8.4 1.1 fusion.30
  9.6 15.0 %all_to_all.29 = bf16[24,8,512]{2,0,1:T(8,128)(2,1)S(1)} all-to-all(bf16[24,8,512]{2,0,1:T(8,128)(2,1)S(1)} %bitcast.61), channel_id=1, replica_groups=mesh['ep'=8,'tp'=4] {'ep'}, dimensions={1} | all-to-all | bytes 393216 | tf_op jit(solution)/shard_map/all_to_all | solution.py:49
  24.6 2.7 convolution_convert_fusion.3
  27.3 1.0 fusion.48
  28.4 1.0 fusion.27
  29.4 0.1 copy.68
  29.5 0.1 copy.73
  29.6 0.1 reshape.151
  29.9 0.2 select_reduce_fusion
  30.1 58.6 %reduce-scatter.4.cloned.1.call-done = bf16[24,1536]{1,0:T(8,128)(2,1)} async-done(((bf16[192,1536]{1,0:T(8,128)(2,1)}), bf16[24,1536]{1,0:T(8,128)(2,1)}) %reduce-scatter.4.cloned.1.call-update) | async-done | bytes 73744 | tf_op jit(solution)/shard_map/reduce_scatter | solution.py:51
  88.7 0.8 fusion.58
  89.5 0.1 multiply_reduce_fusion.3
  89.7 0.1 broadcast_multiply_fusion
  89.8 8.1 %fusion.59 = f32[24,4,1,128]{3,2,1,0:T(1,128)S(1)} fusion(f32[24,4,128,1]{2,3,1,0:T(1,128)S(1)} %bitcast.62, f32[24,4,128,128]{3,2,1,0:T(8,128)} %param.23), kind=kOutput, calls=%fused_computation.93 | convolution fusion | flops 18874368 | bytes 6389760 | tf_op jit(solution)/shard_map/bhk,bhkv->bhv/dot_general | solution.py:73
  97.9 0.1 subtract_multiply_fusion
  98.0 3.9 %multiply_add_fusion = f32[24,4,128,128]{3,2,1,0:T(8,128)} fusion(f32[24,4,128,128]{3,2,1,0:T(8,128)S(1)} %copy-done.1, f32[24,4,128]{2,1,0:T(4,128)S(1)} %subtract_multiply_fusion, f32[24,4,128]{2,1,0:T(4,128)S(1)} %broadcast_multiply_fusion, f32[24,4]{1,0:T(8,128)S(1)} %copy.67), kind=kLoop, calls=%fused_computation.1 | loop fusion | flops 4718592 | bytes 12681600 | tf_op jit(solution)/shard_map/add | solution.py:76
  101.9 0.1 multiply_reduce_fusion.4
  102.0 0.1 multiply_multiply_fusion
  102.2 7.5 %fusion.60 = f32[24,4,1,128]{3,2,1,0:T(1,128)S(1)} fusion(f32[24,4,128,1]{2,3,1,0:T(1,128)S(1)} %bitcast.65, f32[24,4,128,128]{3,2,1,0:T(8,128)} %multiply_add_fusion), kind=kOutput, calls=%fused_computation.94 | convolution fusion | flops 18874368 | bytes 6389760 | tf_op jit(solution)/shard_map/bhk,bhkv->bhv/dot_general | solution.py:78
  109.6 0.1 multiply_reduce_fusion.2
  109.8 0.1 multiply_convert_fusion.1
  109.9 0.7 convolution_convert_fusion.2
  110.6 8.6 %all-gather = bf16[96,4096]{1,0:T(8,128)(2,1)S(1)} all-gather(bf16[24,4096]{1,0:T(8,128)(2,1)S(1)} %convolution_convert_fusion.2), channel_id=2, replica_groups=mesh['ep'=8,'tp'=4] {'tp'}, dimensions={0}, use_global_device_ids=true | all-gather | bytes 983040 | tf_op jit(solution)/shard_map/all_gather | solution.py:81
  119.2 0.2 reduce_sum.92
  119.3 0.9 convert_add_fusion
  120.3 0.1 multiply_convert_fusion
  120.4 0.3 broadcast_in_dim.10
  120.7 0.2 reshape.152
  120.9 0.3 convolution_convert_fusion.1
  121.2 1.2 reshape.153
  122.4 3.6 %all-to-all-start.1 = ((bf16[8,12,4096]{2,1,0:T(8,128)(2,1)}), bf16[8,12,4096]{2,1,0:T(8,128)(2,1)S(1)}, u32[]{:S(2)}, u32[]{:S(2)}) async-start(bf16[8,12,4096]{2,1,0:T(8,128)(2,1)} %reshape.153), calls=%async_computation.3 | async-start | bytes 2097152 | tf_op jit(solution)/shard_map/all_to_all | solution.py:120
  126.1 47.3 %all_gather.11 = bf16[192,1024]{1,0:T(8,128)(2,1)S(1)} all-gather(bf16[24,1024]{1,0:T(8,128)(2,1)S(1)} %constant_dynamic-slice_fusion), channel_id=1, replica_groups=mesh['ep'=8,'tp'=4] {'ep'}, dimensions={0}, use_global_device_ids=true | all-gather | bytes 442368 | tf_op jit(solution)/shard_map/all_gather | solution.py:91
  173.4 2.9 fusion.14
  176.4 2.0 fusion.7
  178.4 3.9 %convolution_convert_fusion = bf16[8,12,4096]{2,1,0:T(8,128)(2,1)} fusion(bf16[1,256,4096]{2,1,0:T(8,128)(2,1)S(1)} %copy-done, bf16[8,12,4096]{2,1,0:T(8,128)(2,1)S(1)} %all-to-all-done.1, bf16[1,4096,256]{2,1,0:T(8,128)(2,1)} %param.38, f32[8,12,256]{2,1,0:T(8,128)S(1)} %fusion.7), kind=kOutput, calls=%fused_computation.2 | convolution fusion | flops 403193856 | bytes 5865472 | tf_op jit(solution)/shard_map/snf,fd->snd/dot_general | solution.py:126
  182.7 24.8 %all-reduce.2.cloned.1.call-done = bf16[192,1024]{1,0:T(8,128)(2,1)} async-done(((bf16[192,1024]{1,0:T(8,128)(2,1)}), bf16[192,1024]{1,0:T(8,128)(2,1)}) %all-reduce.2.cloned.1.call-update) | async-done | bytes 393232 | tf_op jit(solution)/shard_map/psum | solution.py:95
  207.5 1.1 convert_element_type.73
  208.6 2.4 convolution_convert_fusion.4
  211.1 0.1 mul.260
  211.2 23.7 %reduce-scatter.8.cloned.1.call-done = bf16[8,12,1024]{2,1,0:T(8,128)(2,1)} async-done(((bf16[8,12,4096]{2,1,0:T(8,128)(2,1)}), bf16[8,12,1024]{2,1,0:T(8,128)(2,1)}) %reduce-scatter.8.cloned.1.call-update) | async-done | bytes 196624 | tf_op jit(solution)/shard_map/reduce_scatter | solution.py:129
  234.8 5.5 %all-to-all-start.2 = ((bf16[8,12,1024]{2,1,0:T(8,128)(2,1)}), bf16[8,12,1024]{2,1,0:T(8,128)(2,1)S(1)}, u32[]{:S(2)}, u32[]{:S(2)}) async-start(bf16[8,12,1024]{2,1,0:T(8,128)(2,1)} %reduce-scatter.8.cloned.1.call-done), calls=%async_computation.5 | async-start | bytes 524288 | tf_op jit(solution)/shard_map/all_to_all | solution.py:132
  240.3 0.1 copy.75
  240.6 9.1 %all-to-all-done.2 = bf16[8,12,1024]{2,1,0:T(8,128)(2,1)S(1)} async-done(((bf16[8,12,1024]{2,1,0:T(8,128)(2,1)}), bf16[8,12,1024]{2,1,0:T(8,128)(2,1)S(1)}, u32[]{:S(2)}, u32[]{:S(2)}) %all-to-all-start.2) | async-done | bytes 196640 | tf_op jit(solution)/shard_map/all_to_all | solution.py:132
  249.7 0.7 gather_fusion
  250.4 0.4 multiply_reduce_fusion.1
  250.8 49.3 %reduce-scatter.6.cloned.1.call-done = bf16[24,1024]{1,0:T(8,128)(2,1)} async-done(((bf16[192,1024]{1,0:T(8,128)(2,1)}), bf16[24,1024]{1,0:T(8,128)(2,1)}) %reduce-scatter.6.cloned.1.call-update) | async-done | bytes 49168 | tf_op jit(solution)/shard_map/reduce_scatter | solution.py:99
  300.1 1.6 add_convert_fusion
  (59 shorter events, 1.2 us)
Async XLA Ops:
  7.2 171.3 %copy-start = (bf16[1,256,4096]{2,1,0:T(8,128)(2,1)S(1)}, bf16[1,256,4096]{2,1,0:T(8,128)(2,1)}, u32[]{:S(2)}) copy-start(bf16[1,256,4096]{2,1,0:T(8,128)(2,1)} %param.39) | copy-start | bytes 6291460
  7.2 81.6 %reduce-scatter.4.cloned.1.call-start = ((), (), s32[]{:S(2)}) async-start(), calls=%async_computation.6 | async-start | bytes 663552 | tf_op jit(solution)/shard_map/reduce_scatter | solution.py:51
  9.5 17.8 %copy-start.10 = (f32[4]{0:T(128)S(1)}, f32[4]{0:T(128)}, u32[]{:S(2)}) copy-start(f32[4]{0:T(128)} %param.30) | copy-start | bytes 52
  9.5 20.0 %copy-start.5 = (s32[24,2]{0,1:T(2,128)S(1)}, s32[24,2]{0,1:T(2,128)}, u32[]{:S(2)}) copy-start(s32[24,2]{0,1:T(2,128)} %param.34) | copy-start | bytes 580
  89.8 8.2 %copy-start.1 = (f32[24,4,128,128]{3,2,1,0:T(8,128)S(1)}, f32[24,4,128,128]{3,2,1,0:T(8,128)}, u32[]{:S(2)}) copy-start(f32[24,4,128,128]{3,2,1,0:T(8,128)} %param.23) | copy-start | bytes 18874372
  102.1 7.6 %copy-start.8 = (f32[128]{0:T(128)S(1)}, f32[128]{0:T(128)}, u32[]{:S(2)}) copy-start(f32[128]{0:T(128)} %param.31) | copy-start | bytes 1540
  102.1 7.7 %copy-start.2 = (bf16[512,4096]{1,0:T(8,128)(2,1)S(1)}, bf16[512,4096]{1,0:T(8,128)(2,1)}, u32[]{:S(2)}) copy-start(bf16[512,4096]{1,0:T(8,128)(2,1)} %param.32) | copy-start | bytes 12582916
  109.9 9.4 %copy-start.3 = (bf16[24,4096]{1,0:T(8,128)(2,1)S(1)}, bf16[24,4096]{1,0:T(8,128)(2,1)}, u32[]{:S(2)}) copy-start(bf16[24,4096]{1,0:T(8,128)(2,1)} %param.22) | copy-start | bytes 589828
  109.9 10.4 %copy-start.4 = (f32[4096]{0:T(1024)S(1)}, f32[4096]{0:T(1024)}, u32[]{:S(2)}) copy-start(f32[4096]{0:T(1024)} %param.33) | copy-start | bytes 49156
  122.4 54.0 %all-to-all-start.1 = ((bf16[8,12,4096]{2,1,0:T(8,128)(2,1)}), bf16[8,12,4096]{2,1,0:T(8,128)(2,1)S(1)}, u32[]{:S(2)}, u32[]{:S(2)}) async-start(bf16[8,12,4096]{2,1,0:T(8,128)(2,1)} %reshape.153), calls=%async_computation.3 | async-start | bytes 2097152 | tf_op jit(solution)/shard_map/all_to_all | solution.py:120
  126.0 81.4 %all-reduce.2.cloned.1.call-start = ((), (), s32[]{:S(2)}) async-start(), calls=%async_computation.7 | async-start | bytes 786432 | tf_op jit(solution)/shard_map/psum | solution.py:95
  176.3 58.5 %reduce-scatter.8.cloned.1.call-start = ((), (), s32[]{:S(2)}) async-start(), calls=%async_computation.9 | async-start | bytes 1310720 | tf_op jit(solution)/shard_map/reduce_scatter | solution.py:129
  178.4 4.2 %copy-start.7 = (f32[24,2]{0,1:T(2,128)S(1)}, f32[24,2]{0,1:T(2,128)}, u32[]{:S(2)}) copy-start(f32[24,2]{0,1:T(2,128)} %param.36) | copy-start | bytes 580
  178.4 4.2 %copy-start.9 = (f32[24]{0:T(128)S(1)}, f32[24]{0:T(128)}, u32[]{:S(2)}) copy-start(f32[24]{0:T(128)} %param.35) | copy-start | bytes 292
  182.4 58.2 %copy-start.6 = (f32[1024]{0:T(1024)S(1)}, f32[1024]{0:T(1024)}, u32[]{:S(2)}) copy-start(f32[1024]{0:T(1024)} %param.43) | copy-start | bytes 12292
  182.4 117.7 %reduce-scatter.6.cloned.1.call-start = ((), (), s32[]{:S(2)}) async-start(), calls=%async_computation.8 | async-start | bytes 442368 | tf_op jit(solution)/shard_map/reduce_scatter | solution.py:99
  234.8 14.8 %all-to-all-start.2 = ((bf16[8,12,1024]{2,1,0:T(8,128)(2,1)}), bf16[8,12,1024]{2,1,0:T(8,128)(2,1)S(1)}, u32[]{:S(2)}, u32[]{:S(2)}) async-start(bf16[8,12,1024]{2,1,0:T(8,128)(2,1)} %reduce-scatter.8.cloned.1.call-done), calls=%async_computation.5 | async-start | bytes 524288 | tf_op jit(solution)/shard_map/all_to_all | solution.py:132
Sparse Core Ops, SparseCore 0:
  27.4 61.2 reduce-scatter.3
  176.4 30.9 all-reduce.1
  210.0 24.7 reduce-scatter.7
  238.0 62.1 reduce-scatter.5
